TPU v7x, 512 devices: a whole 4x4x16 slice. The times are simulated.
512 devices in a mesh: gr: 2 (over z_hi), fs: 32 (over z_lo, y), tp: 8 (over x, core).
Axes of the slice: x: 4, y: 4, z: 16 (z_hi: 2, z_lo: 8; z = z_hi * 8 + z_lo), core: 2. Of those that a mesh axis runs over, the one named last changes fastest.
Arguments:
- tokens: bfloat16 [24576, 2048], P(('gr', 'fs')), may hold values from -6 to 6
- route_ids: int32 [24576, 2], P(('gr', 'fs')), may hold values from 0 to 31, as said below
- route_weights: float32 [24576, 2], P(('gr', 'fs')), may hold values from 0.1 to 1
- norm_gain: float32 [2048], P(('gr', 'fs')), may hold values from 0.1 to 1.9
- gate_weight: float32 [32, 2048, 1024], P(None, ('gr', 'fs'), 'tp'), may hold values from -0.125 to 0.125
- up_weight: float32 [32, 2048, 1024], P(None, ('gr', 'fs'), 'tp'), may hold values from -0.125 to 0.125
- down_weight: float32 [32, 1024, 2048], P(None, ('gr', 'fs'), 'tp'), may hold values from -0.1875 to 0.1875
Outputs:
- gate_new: bfloat16 [32, 2048, 1024], P('fs', None, 'tp')
- up_new: bfloat16 [32, 2048, 1024], P('fs', None, 'tp')
- down_new: bfloat16 [32, 1024, 2048], P('fs', 'tp')
- mixed: bfloat16 [24576, 2048], P(('gr', 'fs'), 'tp')
Inputs may be any that keep to these rules, and one draw needn't show every extreme that they name: `route_ids`: each row names two different experts of one group (expert e belongs to group e // 8); in each device's block of 384 rows every expert is named by exactly 24 rows.
All inputs are finite; a program needn't handle non-finite values.
Results may differ from a plain program's by a relative error of at most 0.015.
Values may be sent and summed in bfloat16 or wider, within the bound.
A program may use at most 64 MiB of HBM per device.

v0:
```python
import jax
import jax.numpy as jnp
from jax import lax
from jax.sharding import Mesh
from jax.sharding import PartitionSpec as P

TP = ("tp_0", "tp_1")


def side_by_side(arrays, axis, split_dim, concat_dim, along):
    ends, at = ([], 0)
    for a in arrays[:-1]:
        at += a.shape[along]
        ends.append(at)
    both = jnp.concatenate(arrays, axis=along)
    return tuple(
        jnp.split(
            lax.all_to_all(both, axis, split_axis=split_dim, concat_axis=concat_dim, tiled=True),
            ends,
            axis=along,
        )
    )


def in_one_piece(arrays, axis, dim, along):
    ends, at = ([], 0)
    for a in arrays[:-1]:
        at += a.shape[along]
        ends.append(at)
    both = jnp.concatenate(arrays, axis=along)
    return tuple(jnp.split(lax.all_gather(both, axis, axis=dim, tiled=True), ends, axis=along))


def split_up(array, dim, devices):
    before, after = (array.shape[:dim], array.shape[dim + 1 :])
    return jnp.moveaxis(array.reshape(*before, devices, -1, *after), dim, 0)


def laid_out(pieces, dim):
    pieces = jnp.moveaxis(pieces, 0, dim)
    lengths = pieces.shape
    return pieces.reshape(*lengths[:dim], lengths[dim] * lengths[dim + 1], *lengths[dim + 2 :])


def exchange_in_order(pieces, axes, turns):
    inside = pieces.shape[1:]
    whole = pieces.reshape(*(lax.axis_size(a) for a in axes), *inside)
    for k in turns:
        whole = lax.all_to_all(whole, axes[k], k, k, tiled=True)
    return whole.reshape(-1, *inside)


def exchange_by_axis(array, axes, turns, split_dim, concat_dim):
    pieces = split_up(array, split_dim, lax.axis_size(axes))
    return laid_out(exchange_in_order(pieces, axes, turns), concat_dim)


def local(tokens, route_ids, route_weights, norm_gain, gate_weight, up_weight, down_weight):
    gate_folded = (gate_weight * norm_gain[None, :, None]).astype(jnp.bfloat16)
    up_folded = (up_weight * norm_gain[None, :, None]).astype(jnp.bfloat16)
    down_rounded = down_weight.astype(jnp.bfloat16)
    moved = (
        *side_by_side((gate_folded, up_folded), "fs", 0, 1, 2),
        lax.all_to_all(down_rounded, "fs", split_axis=0, concat_axis=1, tiled=True),
    )
    gate_new, up_new, down_whole = (
        *in_one_piece((moved[0], moved[1]), "gr", 1, 0),
        lax.all_gather(moved[2], "gr", axis=1, tiled=True),
    )
    down_new = exchange_by_axis(down_whole, TP, (1, 0), 1, 2)
    tok = tokens.shape[0]
    width = tokens.shape[1]
    experts = gate_weight.shape[0]
    cap = 2 * tok // experts
    flat_ids = route_ids.reshape(-1)
    onehot = (flat_ids[:, None] == jnp.arange(experts, dtype=jnp.int32)[None, :]).astype(jnp.int32)
    slot = jnp.sum(jnp.cumsum(onehot, axis=0) * onehot, axis=1) - 1
    position = flat_ids * cap + slot
    source = (
        jnp.zeros((experts * cap,), jnp.int32)
        .at[position]
        .set(jnp.arange(2 * tok, dtype=jnp.int32) // 2)
    )
    widened = tokens.astype(jnp.float32)
    normed = (
        widened * lax.rsqrt(jnp.mean(widened * widened, axis=-1, keepdims=True) + 1e-06)
    ).astype(jnp.bfloat16)
    outgoing = normed[source].reshape(experts, cap, width)
    received = lax.all_to_all(outgoing, "fs", split_axis=0, concat_axis=0, tiled=True)
    senders, count, _ = received.shape
    rows = received.reshape(senders * count, width)
    first = jnp.dot(rows, gate_new[0], preferred_element_type=jnp.float32)
    second = jnp.dot(rows, up_new[0], preferred_element_type=jnp.float32)
    hidden = (jax.nn.silu(first) * second).astype(jnp.bfloat16)
    hidden_width = hidden.shape[1]
    down_local = down_whole[0]
    out_columns = down_local.shape[1]
    row_count = hidden.shape[0]
    piece = lax.all_gather(hidden, TP, axis=1, tiled=True)
    piece_width = piece.shape[1]
    blocks = piece_width // hidden_width
    partials = jnp.einsum(
        "mbf,bfd->bmd",
        piece.reshape(row_count, blocks, hidden_width),
        down_local.reshape(blocks, hidden_width, out_columns),
        preferred_element_type=jnp.float32,
    ).astype(jnp.bfloat16)
    total = jnp.sum(partials.astype(jnp.float32), axis=0)
    summed = total.reshape(senders, count, out_columns)
    returned = lax.all_to_all(
        summed.astype(jnp.bfloat16), "fs", split_axis=0, concat_axis=0, tiled=True
    )
    columns = returned.shape[2]
    route_out = returned.reshape(experts * cap, columns)[position].reshape(tok, 2, columns)
    mixed = jnp.sum(route_weights[:, :, None] * route_out.astype(jnp.float32), axis=1).astype(
        jnp.bfloat16
    )
    return (gate_new, up_new, down_new, mixed)


def solution(mesh):
    torus = Mesh(
        mesh.devices.reshape(mesh.shape["gr"], mesh.shape["fs"], 4, 2), ("gr", "fs", "tp_0", "tp_1")
    )
    placed = (
        P(("gr", "fs"), None),
        P(("gr", "fs"), None),
        P(("gr", "fs"), None),
        P(("gr", "fs")),
        P(None, ("gr", "fs"), TP),
        P(None, ("gr", "fs"), TP),
        P(None, ("gr", "fs"), TP),
    )
    return jax.shard_map(
        local,
        mesh=torus,
        in_specs=placed,
        out_specs=(P("fs", None, TP), P("fs", None, TP), P("fs", TP, None), P(("gr", "fs"), TP)),
        check_vma=False,
    )
```

profile of v0, /device:TPU:2, one launch (start us, length us, event | category | flops | bytes accessed | tf_op | source)
XLA Modules:
  0.0 370.6 jit_solution(3223288350482646378)
XLA Ops:
  7.2 1.5 multiply_convert_fusion.1
  8.7 0.9 pad_maximum_fusion
  9.6 15.7 %all-to-all-start = ((bf16[32,32,256]{2,1,0:T(8,128)(2,1)}), bf16[32,32,256]{2,1,0:T(8,128)(2,1)}, u32[]{:S(2)}, u32[]{:S(2)}) async-start(bf16[32,32,256]{2,1,0:T(8,128)(2,1)} %pad_maximum_fusion), calls=%async_computation | async-start | bytes 1048576 | tf_op jit(solution)/shard_map/all_to_all | solution.py:18
  25.7 1.7 reduce-window.6
  27.4 0.3 slice_reduce_fusion
  28.2 3.4 scatter_custom_fusion
  31.6 0.4 fusion
  32.0 0.3 fusion.1
  32.4 4.3 %gather_fusion = bf16[768,2048]{1,0:T(8,128)(2,1)} fusion(bf16[384,2048]{1,0:T(8,128)(2,1)S(1)} %fusion.1, s32[1024]{0:T(1024)S(1)} %pad_clamp_fusion.1), kind=kCustom, calls=%fused_computation | custom fusion | bytes 6294528 | tf_op jit(solution)/shard_map/gather | solution.py:88
  36.6 18.2 %all-to-all-done = bf16[32,32,256]{2,1,0:T(8,128)(2,1)} async-done(((bf16[32,32,256]{2,1,0:T(8,128)(2,1)}), bf16[32,32,256]{2,1,0:T(8,128)(2,1)}, u32[]{:S(2)}, u32[]{:S(2)}) %all-to-all-start) | async-done | bytes 524320 | tf_op jit(solution)/shard_map/all_to_all | solution.py:18
  54.8 6.1 %all-to-all-start.4 = ((bf16[32,24,2048]{2,1,0:T(8,128)(2,1)}), bf16[32,24,2048]{2,1,0:T(8,128)(2,1)S(1)}, u32[]{:S(2)}, u32[]{:S(2)}) async-start(bf16[32,24,2048]{2,1,0:T(8,128)(2,1)} %bitcast.48), calls=%async_computation.4 | async-start | bytes 6291456 | tf_op jit(solution)/shard_map/all_to_all | solution.py:89
  61.0 1.1 fusion.18
  62.1 0.8 pad_maximum_fusion.1
  63.0 66.8 %all-gather.3.cloned.1.call-done = bf16[2,2048,128]{2,1,0:T(8,128)(2,1)} async-done(((bf16[2,1024,128]{2,1,0:T(8,128)(2,1)}), bf16[2,2048,128]{2,1,0:T(8,128)(2,1)}) %all-gather.3.cloned.1.call-update) | async-done | bytes 1048592 | tf_op jit(solution)/shard_map/all_gather | solution.py:31
  129.8 2.2 fusion.17
  132.0 114.4 %all-to-all-done.4 = bf16[32,24,2048]{2,1,0:T(8,128)(2,1)S(1)} async-done(((bf16[32,24,2048]{2,1,0:T(8,128)(2,1)}), bf16[32,24,2048]{2,1,0:T(8,128)(2,1)S(1)}, u32[]{:S(2)}, u32[]{:S(2)}) %all-to-all-start.4) | async-done | bytes 3145760 | tf_op jit(solution)/shard_map/all_to_all | solution.py:89
  246.4 2.1 fusion.6
  248.5 1.7 fusion.4
  250.2 1.1 convert_element_type.42
  251.3 26.3 %all_to_all.44 = bf16[32,16,256]{2,1,0:T(8,128)(2,1)S(1)} all-to-all(bf16[32,16,256]{2,1,0:T(8,128)(2,1)S(1)} %convert_element_type.42), channel_id=1, replica_groups=mesh['gr'=2,'fs'=32,'tp_0'=4,'tp_1'=2] {'fs'}, dimensions={0} | all-to-all | bytes 524288 | tf_op jit(solution)/shard_map/all_to_all | solution.py:64
  277.6 29.7 %all_gather.10 = bf16[1,1024,256]{2,1,0:T(8,128)(2,1)S(1)} all-gather(bf16[1,512,256]{2,1,0:T(8,128)(2,1)S(1)} %bitcast.52), channel_id=1, replica_groups=mesh['gr'=2,'fs'=32,'tp_0'=4,'tp_1'=2] {'gr'}, dimensions={1}, use_global_device_ids=true | all-gather | bytes 786432 | tf_op jit(solution)/shard_map/all_gather | solution.py:68
  307.3 4.2 %all_to_all.45 = bf16[4,2,1,128,256]{4,3,0,2,1:T(8,128)(2,1)S(1)} all-to-all(bf16[4,2,1,128,256]{4,3,0,2,1:T(8,128)(2,1)S(1)} %copy.29), channel_id=1, replica_groups=mesh['gr'=2,'fs'=32,'tp_0'=4,'tp_1'=2] {'tp_1'}, dimensions={1} | all-to-all | bytes 1048576 | tf_op jit(solution)/shard_map/all_to_all | solution.py:49
  311.5 0.8 copy.30
  312.3 5.0 %all-to-all-start.3 = ((bf16[4,2,1,128,256]{4,3,1,2,0:T(8,128)(2,1)}), bf16[4,2,1,128,256]{4,3,1,2,0:T(8,128)(2,1)S(1)}, u32[]{:S(2)}, u32[]{:S(2)}) async-start(bf16[4,2,1,128,256]{4,3,1,2,0:T(8,128)(2,1)} %copy.30), calls=%async_computation.3 | async-start | bytes 1048576 | tf_op jit(solution)/shard_map/all_to_all | solution.py:49
  317.3 3.2 convert_reduce_fusion
  320.5 5.1 %all-to-all-done.3 = bf16[4,2,1,128,256]{4,3,1,2,0:T(8,128)(2,1)S(1)} async-done(((bf16[4,2,1,128,256]{4,3,1,2,0:T(8,128)(2,1)}), bf16[4,2,1,128,256]{4,3,1,2,0:T(8,128)(2,1)S(1)}, u32[]{:S(2)}, u32[]{:S(2)}) %all-to-all-start.3) | async-done | bytes 524320 | tf_op jit(solution)/shard_map/all_to_all | solution.py:49
  325.6 10.0 %all-to-all-start.5 = ((bf16[32,24,256]{2,1,0:T(8,128)(2,1)}), bf16[32,24,256]{2,1,0:T(8,128)(2,1)S(1)}, u32[]{:S(2)}, u32[]{:S(2)}) async-start(bf16[32,24,256]{2,1,0:T(8,128)(2,1)} %bitcast.11), calls=%async_computation.5 | async-start | bytes 786432 | tf_op jit(solution)/shard_map/all_to_all | solution.py:110
  335.7 0.8 copy.39
  336.6 22.4 %all-to-all-done.5 = bf16[32,24,256]{2,1,0:T(8,128)(2,1)S(1)} async-done(((bf16[32,24,256]{2,1,0:T(8,128)(2,1)}), bf16[32,24,256]{2,1,0:T(8,128)(2,1)S(1)}, u32[]{:S(2)}, u32[]{:S(2)}) %all-to-all-start.5) | async-done | bytes 393248 | tf_op jit(solution)/shard_map/all_to_all | solution.py:110
  359.0 2.6 gather_fusion.1
  361.6 0.4 reshape.105
  362.0 1.7 multiply_reduce_fusion
  (31 shorter events, 1.2 us)
Async XLA Ops:
  7.2 18.1 %copy-start.2 = (s32[384,2]{0,1:T(2,128)S(1)}, s32[384,2]{0,1:T(2,128)}, u32[]{:S(2)}) copy-start(s32[384,2]{0,1:T(2,128)} %param.8) | copy-start | bytes 9220
  7.2 24.4 %copy-start = (bf16[384,2048]{1,0:T(8,128)(2,1)S(1)}, bf16[384,2048]{1,0:T(8,128)(2,1)}, u32[]{:S(2)}) copy-start(bf16[384,2048]{1,0:T(8,128)(2,1)} %param.7) | copy-start | bytes 4718596
  9.6 45.3 %all-to-all-start = ((bf16[32,32,256]{2,1,0:T(8,128)(2,1)}), bf16[32,32,256]{2,1,0:T(8,128)(2,1)}, u32[]{:S(2)}, u32[]{:S(2)}) async-start(bf16[32,32,256]{2,1,0:T(8,128)(2,1)} %pad_maximum_fusion), calls=%async_computation | async-start | bytes 1048576 | tf_op jit(solution)/shard_map/all_to_all | solution.py:18
  54.8 191.6 %all-to-all-start.4 = ((bf16[32,24,2048]{2,1,0:T(8,128)(2,1)}), bf16[32,24,2048]{2,1,0:T(8,128)(2,1)S(1)}, u32[]{:S(2)}, u32[]{:S(2)}) async-start(bf16[32,24,2048]{2,1,0:T(8,128)(2,1)} %bitcast.48), calls=%async_computation.4 | async-start | bytes 6291456 | tf_op jit(solution)/shard_map/all_to_all | solution.py:89
  60.9 68.8 %all-gather.3.cloned.1.call-start = ((), (), s32[]{:S(2)}) async-start(), calls=%async_computation.6 | async-start | bytes 1572864 | tf_op jit(solution)/shard_map/all_gather | solution.py:31
  62.9 254.4 %all-gather.5.cloned.1.call-start = ((), (), s32[]{:S(2)}) async-start(), calls=%async_computation.7 | async-start | bytes 1769472 | tf_op jit(solution)/shard_map/all_gather | solution.py:99
  246.4 2.1 copy-start.1
  312.3 23.3 %copy-start.3 = (f32[384,2]{0,1:T(2,128)S(1)}, f32[384,2]{0,1:T(2,128)}, u32[]{:S(2)}) copy-start(f32[384,2]{0,1:T(2,128)} %param.9) | copy-start | bytes 9220
  312.3 13.3 %all-to-all-start.3 = ((bf16[4,2,1,128,256]{4,3,1,2,0:T(8,128)(2,1)}), bf16[4,2,1,128,256]{4,3,1,2,0:T(8,128)(2,1)S(1)}, u32[]{:S(2)}, u32[]{:S(2)}) async-start(bf16[4,2,1,128,256]{4,3,1,2,0:T(8,128)(2,1)} %copy.30), calls=%async_computation.3 | async-start | bytes 1048576 | tf_op jit(solution)/shard_map/all_to_all | solution.py:49
  325.6 33.4 %all-to-all-start.5 = ((bf16[32,24,256]{2,1,0:T(8,128)(2,1)}), bf16[32,24,256]{2,1,0:T(8,128)(2,1)S(1)}, u32[]{:S(2)}, u32[]{:S(2)}) async-start(bf16[32,24,256]{2,1,0:T(8,128)(2,1)} %bitcast.11), calls=%async_computation.5 | async-start | bytes 786432 | tf_op jit(solution)/shard_map/all_to_all | solution.py:110
Sparse Core Ops, SparseCore 0:
  64.4 65.2 all-gather.2
  250.3 28.7 all-gather.4
where the time goes:
time: 371 us
  waiting for transfers between devices  227 us (61%)
  blocking collectives  60.1 us (16%)
  starting transfers between devices  36.8 us (10%)
  local copies, waits for them, and re-layouts  16.8 us (5%)
  between operations  14.3 us (4%)
  other arithmetic  8.64 us (2%)
  matrix products  6.94 us (2%)
    all_to_all x1, waiting for transfers between devices, local(): lax.all_to_all(outgoing, 'fs', split_axis=0, concat_axis=0, tiled=True)  114 us
    all_gather x1, waiting for transfers between devices, in_one_piece(): lax.all_gather(both, axis, axis=dim, tiled=True)  66.8 us
    all_gather x1, blocking collectives, local(): lax.all_gather(moved[2], 'gr', axis=1, tiled=True)  29.7 us
    all_to_all x1, blocking collectives, local(): lax.all_to_all(down_rounded, 'fs', split_axis=0, concat_axis=1, tiled=True)  26.3 us
    all_to_all x1, waiting for transfers between devices, local(): lax.all_to_all(summed.astype(jnp.bfloat16), 'fs', split_axis=0, concat_ax...  22.4 us
    all_to_all x1, waiting for transfers between devices, side_by_side(): lax.all_to_all(both, axis, split_axis=split_dim, concat_axis=concat_dim,...  18.2 us
    all_to_all x1, starting transfers between devices, side_by_side(): lax.all_to_all(both, axis, split_axis=split_dim, concat_axis=concat_dim,...  15.7 us
    all_to_all x1, starting transfers between devices, local(): lax.all_to_all(summed.astype(jnp.bfloat16), 'fs', split_axis=0, concat_ax...  9.96 us
  transfers between devices with their start and end apart: 6, of which 5 were waited for; matrix products, arithmetic and copies ran while one was open for 6% of the time, Pallas kernels for 0%

commit v1 on v0

--- a/solution.py
+++ b/solution.py
@@ -3,6 +3,7 @@
 from jax import lax
 from jax.sharding import Mesh
 from jax.sharding import PartitionSpec as P
+from jax.lax import all_to_all, axis_size
 
 TP = ("tp_0", "tp_1")
 
@@ -61,7 +62,9 @@
     down_rounded = down_weight.astype(jnp.bfloat16)
     moved = (
         *side_by_side((gate_folded, up_folded), "fs", 0, 1, 2),
-        lax.all_to_all(down_rounded, "fs", split_axis=0, concat_axis=1, tiled=True),
+        jnp.concatenate(
+            all_to_all(jnp.stack(jnp.split(down_rounded, axis_size("fs"), 0)), "fs", 0, 0), axis=1
+        ),
     )
     gate_new, up_new, down_whole = (
         *in_one_piece((moved[0], moved[1]), "gr", 1, 0),

time: 371 us -> 375 us (1.011)
  local copies, waits for them, and re-layouts: 16.8 us -> 24.7 us
  waiting for transfers between devices: 227 us -> 222 us
    unnamed x10 -> x43, local copies, waits for them, and re-layouts: 0.29 us -> 7.57 us
    all_gather x1, waiting for transfers between devices: 66.8 us -> 62.3 us  [in_one_piece(): lax.all_gather(both, axis, axis=dim, tiled=True)]
  transfers between devices with their start and end apart: 6 -> 6, of which waited for: 5 -> 5; matrix products, arithmetic and copies ran while one was open for 6% -> 8% of each run, Pallas kernels for 0% -> 0%
where the time goes in v1:
time: 375 us; the launch traced here: 374 us
  waiting for transfers between devices  222 us (59%)
  blocking collectives  60.3 us (16%)
  starting transfers between devices  36.8 us (10%)
  local copies, waits for them, and re-layouts  24.7 us (7%)
  between operations  14.4 us (4%)
  other arithmetic  8.64 us (2%)
  matrix products  6.94 us (2%)
    all_to_all x1, waiting for transfers between devices, local(): lax.all_to_all(outgoing, 'fs', split_axis=0, concat_axis=0, tiled=True)  114 us
    all_gather x1, waiting for transfers between devices, in_one_piece(): lax.all_gather(both, axis, axis=dim, tiled=True)  62.3 us
    all_gather x1, blocking collectives, local(): lax.all_gather(moved[2], 'gr', axis=1, tiled=True)  29.7 us
    all_to_all x1, blocking collectives, local(): all_to_all(jnp.stack(jnp.split(down_rounded, axis_size('fs'), 0)), 'fs',...  26.5 us
    all_to_all x1, waiting for transfers between devices, local(): lax.all_to_all(summed.astype(jnp.bfloat16), 'fs', split_axis=0, concat_ax...  22.4 us
    all_to_all x1, waiting for transfers between devices, side_by_side(): lax.all_to_all(both, axis, split_axis=split_dim, concat_axis=concat_dim,...  18.2 us
    all_to_all x1, starting transfers between devices, side_by_side(): lax.all_to_all(both, axis, split_axis=split_dim, concat_axis=concat_dim,...  15.7 us
    all_to_all x1, starting transfers between devices, local(): lax.all_to_all(summed.astype(jnp.bfloat16), 'fs', split_axis=0, concat_ax...  9.97 us
  transfers between devices with their start and end apart: 6, of which 5 were waited for; matrix products, arithmetic and copies ran while one was open for 8% of the time, Pallas kernels for 0%

profile of v1, /device:TPU:2, one launch (start us, length us, event | category | flops | bytes accessed | tf_op | source)
XLA Modules:
  0.0 373.9 jit_solution(5655376793444644242)
XLA Ops:
  7.2 1.5 multiply_convert_fusion.1
  8.7 0.9 pad_maximum_fusion
  9.6 15.7 %all-to-all-start = ((bf16[32,32,256]{2,1,0:T(8,128)(2,1)}), bf16[32,32,256]{2,1,0:T(8,128)(2,1)}, u32[]{:S(2)}, u32[]{:S(2)}) async-start(bf16[32,32,256]{2,1,0:T(8,128)(2,1)} %pad_maximum_fusion), calls=%async_computation | async-start | bytes 1048576 | tf_op jit(solution)/shard_map/all_to_all | solution.py:19
  25.7 1.7 reduce-window.6
  28.2 3.4 scatter_custom_fusion
  32.4 4.3 %gather_fusion = bf16[768,2048]{1,0:T(8,128)(2,1)} fusion(bf16[384,2048]{1,0:T(8,128)(2,1)S(1)} %fusion.1, s32[1024]{0:T(1024)S(1)} %pad_clamp_fusion.1), kind=kCustom, calls=%fused_computation | custom fusion | bytes 6294528 | tf_op jit(solution)/shard_map/gather | solution.py:91
  36.6 18.2 %all-to-all-done = bf16[32,32,256]{2,1,0:T(8,128)(2,1)} async-done(((bf16[32,32,256]{2,1,0:T(8,128)(2,1)}), bf16[32,32,256]{2,1,0:T(8,128)(2,1)}, u32[]{:S(2)}, u32[]{:S(2)}) %all-to-all-start) | async-done | bytes 524320 | tf_op jit(solution)/shard_map/all_to_all | solution.py:19
  54.8 6.1 %all-to-all-start.4 = ((bf16[32,24,2048]{2,1,0:T(8,128)(2,1)}), bf16[32,24,2048]{2,1,0:T(8,128)(2,1)S(1)}, u32[]{:S(2)}, u32[]{:S(2)}) async-start(bf16[32,24,2048]{2,1,0:T(8,128)(2,1)} %bitcast.176), calls=%async_computation.4 | async-start | bytes 6291456 | tf_op jit(solution)/shard_map/all_to_all | solution.py:92
  61.0 1.1 convert_element_type.42
  62.3 0.7 copy-done.2
  63.0 1.1 fusion.18
  64.0 0.8 pad_maximum_fusion.1
  67.9 62.3 %all-gather.3.cloned.1.call-done = bf16[2,2048,128]{2,1,0:T(8,128)(2,1)} async-done(((bf16[2,1024,128]{2,1,0:T(8,128)(2,1)}), bf16[2,2048,128]{2,1,0:T(8,128)(2,1)}) %all-gather.3.cloned.1.call-update) | async-done | bytes 1048592 | tf_op jit(solution)/shard_map/all_gather | solution.py:32
  130.2 2.2 fusion.17
  132.4 114.0 %all-to-all-done.4 = bf16[32,24,2048]{2,1,0:T(8,128)(2,1)S(1)} async-done(((bf16[32,24,2048]{2,1,0:T(8,128)(2,1)}), bf16[32,24,2048]{2,1,0:T(8,128)(2,1)S(1)}, u32[]{:S(2)}, u32[]{:S(2)}) %all-to-all-start.4) | async-done | bytes 3145760 | tf_op jit(solution)/shard_map/all_to_all | solution.py:92
  246.4 2.1 fusion.6
  248.5 1.7 fusion.4
  250.2 0.6 constant_dynamic-update-slice_fusion.6
  250.8 0.6 constant_dynamic-update-slice_fusion.5
  253.8 0.6 constant_dynamic-update-slice_fusion
  254.4 26.5 %all_to_all.37 = bf16[32,1,16,256]{3,2,1,0:T(8,128)(2,1)S(1)} all-to-all(bf16[32,1,16,256]{3,2,1,0:T(8,128)(2,1)} %constant_dynamic-update-slice_fusion), channel_id=1, replica_groups=mesh['gr'=2,'fs'=32,'tp_0'=4,'tp_1'=2] {'fs'}, dimensions={0} | all-to-all | bytes 524288 | tf_op jit(solution)/shard_map/all_to_all | solution.py:66
  280.9 29.7 %all_gather.10 = bf16[1,1024,256]{2,1,0:T(8,128)(2,1)S(1)} all-gather(bf16[1,512,256]{2,1,0:T(8,128)(2,1)S(1)} %bitcast.180), channel_id=1, replica_groups=mesh['gr'=2,'fs'=32,'tp_0'=4,'tp_1'=2] {'gr'}, dimensions={1}, use_global_device_ids=true | all-gather | bytes 786432 | tf_op jit(solution)/shard_map/all_gather | solution.py:71
  310.6 4.2 %all_to_all.38 = bf16[4,2,1,128,256]{4,3,0,2,1:T(8,128)(2,1)S(1)} all-to-all(bf16[4,2,1,128,256]{4,3,0,2,1:T(8,128)(2,1)S(1)} %copy.29), channel_id=1, replica_groups=mesh['gr'=2,'fs'=32,'tp_0'=4,'tp_1'=2] {'tp_1'}, dimensions={1} | all-to-all | bytes 1048576 | tf_op jit(solution)/shard_map/all_to_all | solution.py:50
  314.8 0.8 copy.30
  315.6 5.0 %all-to-all-start.3 = ((bf16[4,2,1,128,256]{4,3,1,2,0:T(8,128)(2,1)}), bf16[4,2,1,128,256]{4,3,1,2,0:T(8,128)(2,1)S(1)}, u32[]{:S(2)}, u32[]{:S(2)}) async-start(bf16[4,2,1,128,256]{4,3,1,2,0:T(8,128)(2,1)} %copy.30), calls=%async_computation.3 | async-start | bytes 1048576 | tf_op jit(solution)/shard_map/all_to_all | solution.py:50
  320.6 3.2 convert_reduce_fusion
  323.8 5.1 %all-to-all-done.3 = bf16[4,2,1,128,256]{4,3,1,2,0:T(8,128)(2,1)S(1)} async-done(((bf16[4,2,1,128,256]{4,3,1,2,0:T(8,128)(2,1)}), bf16[4,2,1,128,256]{4,3,1,2,0:T(8,128)(2,1)S(1)}, u32[]{:S(2)}, u32[]{:S(2)}) %all-to-all-start.3) | async-done | bytes 524320 | tf_op jit(solution)/shard_map/all_to_all | solution.py:50
  328.9 10.0 %all-to-all-start.5 = ((bf16[32,24,256]{2,1,0:T(8,128)(2,1)}), bf16[32,24,256]{2,1,0:T(8,128)(2,1)S(1)}, u32[]{:S(2)}, u32[]{:S(2)}) async-start(bf16[32,24,256]{2,1,0:T(8,128)(2,1)} %bitcast.43), calls=%async_computation.5 | async-start | bytes 786432 | tf_op jit(solution)/shard_map/all_to_all | solution.py:113
  339.0 0.8 copy.39
  339.9 22.4 %all-to-all-done.5 = bf16[32,24,256]{2,1,0:T(8,128)(2,1)S(1)} async-done(((bf16[32,24,256]{2,1,0:T(8,128)(2,1)}), bf16[32,24,256]{2,1,0:T(8,128)(2,1)S(1)}, u32[]{:S(2)}, u32[]{:S(2)}) %all-to-all-start.5) | async-done | bytes 393248 | tf_op jit(solution)/shard_map/all_to_all | solution.py:113
  362.3 2.6 gather_fusion.1
  365.3 1.7 multiply_reduce_fusion
  (65 shorter events, 8.0 us)
Async XLA Ops:
  7.2 18.1 %copy-start.3 = (s32[384,2]{0,1:T(2,128)S(1)}, s32[384,2]{0,1:T(2,128)}, u32[]{:S(2)}) copy-start(s32[384,2]{0,1:T(2,128)} %param.8) | copy-start | bytes 9220
  7.2 24.4 %copy-start = (bf16[384,2048]{1,0:T(8,128)(2,1)S(1)}, bf16[384,2048]{1,0:T(8,128)(2,1)}, u32[]{:S(2)}) copy-start(bf16[384,2048]{1,0:T(8,128)(2,1)} %param.7) | copy-start | bytes 4718596
  9.6 45.3 %all-to-all-start = ((bf16[32,32,256]{2,1,0:T(8,128)(2,1)}), bf16[32,32,256]{2,1,0:T(8,128)(2,1)}, u32[]{:S(2)}, u32[]{:S(2)}) async-start(bf16[32,32,256]{2,1,0:T(8,128)(2,1)} %pad_maximum_fusion), calls=%async_computation | async-start | bytes 1048576 | tf_op jit(solution)/shard_map/all_to_all | solution.py:19
  54.8 191.6 %all-to-all-start.4 = ((bf16[32,24,2048]{2,1,0:T(8,128)(2,1)}), bf16[32,24,2048]{2,1,0:T(8,128)(2,1)S(1)}, u32[]{:S(2)}, u32[]{:S(2)}) async-start(bf16[32,24,2048]{2,1,0:T(8,128)(2,1)} %bitcast.176), calls=%async_computation.4 | async-start | bytes 6291456 | tf_op jit(solution)/shard_map/all_to_all | solution.py:92
  60.9 69.2 %all-gather.3.cloned.1.call-start = ((), (), s32[]{:S(2)}) async-start(), calls=%async_computation.6 | async-start | bytes 1572864 | tf_op jit(solution)/shard_map/all_gather | solution.py:32
  62.3 0.7 copy-start.2
  64.9 255.7 %all-gather.5.cloned.1.call-start = ((), (), s32[]{:S(2)}) async-start(), calls=%async_computation.7 | async-start | bytes 1769472 | tf_op jit(solution)/shard_map/all_gather | solution.py:102
  246.4 2.1 copy-start.1
  315.6 23.3 %copy-start.4 = (f32[384,2]{0,1:T(2,128)S(1)}, f32[384,2]{0,1:T(2,128)}, u32[]{:S(2)}) copy-start(f32[384,2]{0,1:T(2,128)} %param.9) | copy-start | bytes 9220
  315.6 13.3 %all-to-all-start.3 = ((bf16[4,2,1,128,256]{4,3,1,2,0:T(8,128)(2,1)}), bf16[4,2,1,128,256]{4,3,1,2,0:T(8,128)(2,1)S(1)}, u32[]{:S(2)}, u32[]{:S(2)}) async-start(bf16[4,2,1,128,256]{4,3,1,2,0:T(8,128)(2,1)} %copy.30), calls=%async_computation.3 | async-start | bytes 1048576 | tf_op jit(solution)/shard_map/all_to_all | solution.py:50
  328.9 33.4 %all-to-all-start.5 = ((bf16[32,24,256]{2,1,0:T(8,128)(2,1)}), bf16[32,24,256]{2,1,0:T(8,128)(2,1)S(1)}, u32[]{:S(2)}, u32[]{:S(2)}) async-start(bf16[32,24,256]{2,1,0:T(8,128)(2,1)} %bitcast.43), calls=%async_computation.5 | async-start | bytes 786432 | tf_op jit(solution)/shard_map/all_to_all | solution.py:113
Sparse Core Ops, SparseCore 0:
  65.0 65.1 all-gather.2
  250.3 28.7 all-gather.4
